TPU v7x, 256 devices: a whole 4x4x8 slice. The times are simulated.
256 devices in a mesh: ep: 128 (over z, y, x), tp: 2 (over core).
Axes of the slice: x: 4, y: 4, z: 8, core: 2. Of those that a mesh axis runs over, the one named last changes fastest.
Arguments:
- tokens: bfloat16 [65536, 2048], P(('ep', 'tp')), may hold values from -6 to 6
- norm_gain: float32 [2048], replicated, may hold values from 0.1 to 1.9
- expert_ids: int32 [65536, 2], P(('ep', 'tp')), may hold values from 0 to 127, all different within a row; in each aligned block of 256 rows (0 to 255, 256 to 511, ...) at most 6 rows name the same one
- route_weights: float32 [65536, 2], P(('ep', 'tp')), may hold values from 0.2 to 1.2
- expert_gate: bfloat16 [128, 2048, 512], P('ep', None, 'tp'), may hold values from -0.125 to 0.125
- expert_up: bfloat16 [128, 2048, 512], P('ep', None, 'tp'), may hold values from -0.125 to 0.125
- expert_down: bfloat16 [128, 512, 2048], P('ep', 'tp'), may hold values from -0.25 to 0.25
- shared_gate: bfloat16 [2048, 512], P(None, 'tp'), may hold values from -0.125 to 0.125
- shared_up: bfloat16 [2048, 512], P(None, 'tp'), may hold values from -0.125 to 0.125
- shared_down: bfloat16 [512, 2048], P('tp'), may hold values from -0.25 to 0.25
Outputs:
- mixed: bfloat16 [65536, 2048], P(('ep', 'tp'))
Inputs may be any that keep to these rules, and one draw needn't show every extreme that they name: `expert_ids`: each token names 2 different experts. Among the tokens of one device (aligned blocks of 256 rows) no expert is named by more than 6 tokens, and in every block some expert is named by exactly 6.
All inputs are finite; a program needn't handle non-finite values.
Results may differ from a plain program's by a relative error of at most 0.0075.
Values may be sent and summed in bfloat16 or wider, within the bound.
No kernel may reach another device: no remote copies, remote signals or barrier semaphores. Data moves between devices by JAX's collectives and lax.ppermute only.
A program may use at most 64 MiB of HBM per device.

v0:
```python
import jax
import jax.numpy as jnp
from jax import lax
from jax.sharding import PartitionSpec as P

epsilon = 1e-06


def normalize(tokens, norm_gain):
    values = tokens.astype(jnp.float32)
    factor = lax.rsqrt(jnp.mean(values * values, axis=1, keepdims=True) + epsilon)
    return (values * factor * norm_gain[None, :]).astype(jnp.bfloat16)


def round_term(partial_value):
    return lax.optimization_barrier(partial_value.astype(jnp.bfloat16)).astype(jnp.float32)


def gated_rows(row_block, gate_w, up_w):
    gate_value = jnp.dot(row_block, gate_w, preferred_element_type=jnp.float32)
    up_value = jnp.dot(row_block, up_w, preferred_element_type=jnp.float32)
    return (jax.nn.silu(gate_value) * up_value).astype(jnp.bfloat16)


def sliced_term(hidden, down_w):
    return round_term(jnp.dot(hidden, down_w, preferred_element_type=jnp.float32))


def shared_branch(normed, shared_gate, shared_up, shared_down):
    hidden = gated_rows(lax.all_gather(normed, "tp", axis=0, tiled=True), shared_gate, shared_up)
    return lax.psum_scatter(
        sliced_term(hidden, shared_down).astype(jnp.bfloat16), "tp", scatter_dimension=0, tiled=True
    ).astype(jnp.float32)


def body(
    tokens,
    norm_gain,
    expert_ids,
    route_weights,
    expert_gate,
    expert_up,
    expert_down,
    shared_gate,
    shared_up,
    shared_down,
):
    normed = normalize(tokens, norm_gain)
    tok_rows = tokens.shape[0]
    model_width = tokens.shape[1]
    top_count = expert_ids.shape[1]
    ep_size = lax.axis_size("ep")
    experts = expert_gate.shape[0] * ep_size
    capacity = 3 * tok_rows * top_count // (2 * experts)
    assigned = tok_rows * top_count
    gate_one = expert_gate[0]
    up_one = expert_up[0]
    down_one = expert_down[0]
    flat_ids = expert_ids.reshape(-1)
    onehot = (flat_ids[:, None] == jnp.arange(experts, dtype=jnp.int32)[None, :]).astype(
        jnp.bfloat16
    )
    earlier = (jnp.arange(assigned)[:, None] > jnp.arange(assigned)[None, :]).astype(jnp.bfloat16)
    before_count = jnp.dot(earlier, onehot, preferred_element_type=jnp.float32)
    slot_index = jnp.sum(before_count * onehot.astype(jnp.float32), axis=1).astype(jnp.int32)
    position = flat_ids * capacity + slot_index
    owners = (
        jnp.full((experts * capacity,), tok_rows, jnp.int32)
        .at[position]
        .set(jnp.arange(assigned, dtype=jnp.int32) // top_count)
    )
    padded = jnp.concatenate([normed, jnp.zeros((1, model_width), jnp.bfloat16)], axis=0)
    outgoing = padded[owners].reshape(ep_size, capacity, model_width)
    received = lax.all_to_all(outgoing, "ep", split_axis=0, concat_axis=0, tiled=True)
    hidden = gated_rows(
        lax.all_gather(received.reshape(ep_size * capacity, model_width), "tp", axis=0, tiled=True),
        gate_one,
        up_one,
    )
    summed = lax.psum_scatter(
        sliced_term(hidden, down_one).astype(jnp.bfloat16), "tp", scatter_dimension=0, tiled=True
    )
    returned = lax.all_to_all(
        summed.reshape(ep_size, capacity, model_width),
        "ep",
        split_axis=0,
        concat_axis=0,
        tiled=True,
    )
    gathered = returned.reshape(experts * capacity, model_width)[position]
    routed = jnp.sum(
        gathered.reshape(tok_rows, top_count, model_width).astype(jnp.float32)
        * route_weights[:, :, None],
        axis=1,
    )
    shared_out = shared_branch(normed, shared_gate, shared_up, shared_down)
    return (routed + shared_out).astype(jnp.bfloat16)


def solution(mesh):
    placed = (
        P(("ep", "tp"), None),
        P(),
        P(("ep", "tp"), None),
        P(("ep", "tp"), None),
        P("ep", None, "tp"),
        P("ep", None, "tp"),
        P("ep", "tp", None),
        P(None, "tp"),
        P(None, "tp"),
        P("tp", None),
    )
    return jax.shard_map(
        body, mesh=mesh, in_specs=placed, out_specs=P(("ep", "tp"), None), check_vma=False
    )
```

profile of v0, /device:TPU:6, one launch (start us, length us, event | category | flops | bytes accessed | tf_op | source)
XLA Modules:
  0.0 347.6 jit_solution(12503295927482520006)
XLA Ops:
  6.5 0.0 copy-start
  6.5 0.0 copy-start.3
  6.5 0.0 copy-start.4
  6.5 0.0 all-gather.3.cloned.1.call-start
  6.5 1.0 copy.13
  7.5 0.7 broadcast_multiply_fusion
  8.2 1.5 fusion.1
  9.7 0.1 eq.15
  9.9 0.3 fusion.5
  10.2 0.1 copy.12
  10.3 0.1 mul.67
  10.5 2.4 scatter_custom_fusion
  13.0 0.0 copy-done.3
  13.0 0.0 copy-done.4
  13.0 0.3 fusion.3
  13.3 0.0 copy-start.2
  13.3 0.1 concatenate.3
  13.4 4.3 %gather_fusion = bf16[768,2048]{1,0:T(8,128)(2,1)} fusion(bf16[257,2048]{1,0:T(8,128)(2,1)S(1)} %concatenate.3, s32[1024]{0:T(1024)S(1)} %pad_clamp_fusion.1), kind=kCustom, calls=%fused_computation | custom fusion | bytes 6294528 | tf_op jit(solution)/shard_map/gather | solution.py:73
  17.7 0.0 copy-done.2
  17.7 6.2 %reshape.59 = bf16[128,6,2048]{2,1,0:T(8,128)(2,1)} reshape(bf16[768,2048]{1,0:T(8,128)(2,1)} %gather_fusion) | data formatting | bytes 6291456 | tf_op jit(solution)/shard_map/reshape | solution.py:73
  23.9 111.4 %all_to_all.10 = bf16[128,6,2048]{2,1,0:T(8,128)(2,1)} all-to-all(bf16[128,6,2048]{2,1,0:T(8,128)(2,1)} %reshape.59), channel_id=1, replica_groups=mesh['ep'=128,'tp'=2] {'ep'}, dimensions={0} | all-to-all | bytes 6291456 | tf_op jit(solution)/shard_map/all_to_all | solution.py:74
  135.3 6.3 %reshape.60 = bf16[768,2048]{1,0:T(8,128)(2,1)} reshape(bf16[128,6,2048]{2,1,0:T(8,128)(2,1)} %all_to_all.10) | data formatting | bytes 6291456 | tf_op jit(solution)/shard_map/reshape | solution.py:76
  141.7 0.0 copy-start.7
  141.7 0.0 all-gather.3.cloned.1.call-update
  141.7 0.0 copy-start.8
  141.7 0.2 reduce-scatter.3.cloned.1.call-start
  141.9 18.4 %all-gather.3.cloned.1.call-done = bf16[1536,2048]{1,0:T(8,128)(2,1)} async-done(((bf16[768,2048]{1,0:T(8,128)(2,1)}), bf16[1536,2048]{1,0:T(8,128)(2,1)}) %all-gather.3.cloned.1.call-update) | async-done | bytes 6291472 | tf_op jit(solution)/shard_map/all_gather | solution.py:76
  160.3 0.0 copy-done.7
  160.3 5.8 %fusion.9 = f32[1536,256]{1,0:T(8,128)} fusion(bf16[1536,2048]{1,0:T(8,128)(2,1)} %all-gather.3.cloned.1.call-done, bf16[1,2048,256]{2,1,0:T(8,128)(2,1)S(1)} %copy-done.7), kind=kOutput, calls=%fused_computation.20 | convolution fusion | flops 1610612736 | bytes 8912896 | tf_op jit(solution)/shard_map/dot_general | solution.py:20
  166.1 0.0 copy-done
  166.1 0.0 copy-done.8
  166.1 12.3 %convolution_convert_fusion = bf16[1536,2048]{1,0:T(8,128)(2,1)} fusion(bf16[1536,2048]{1,0:T(8,128)(2,1)} %all-gather.3.cloned.1.call-done, f32[1536,256]{1,0:T(8,128)} %fusion.9, bf16[1,256,2048]{2,1,0:T(8,128)(2,1)S(1)} %copy-done, bf16[1,2048,256]{2,1,0:T(8,128)(2,1)S(1)} %copy-done.8), kind=kOutput, calls=%fused_computation.3 | convolution fusion | flops 3226730496 | bytes 16252928 | tf_op jit(solution)/shard_map/dot_general | solution.py:26
  178.4 0.0 reduce-scatter.3.cloned.1.call-update
  178.4 0.0 all-gather.5.cloned.1.call-start
  178.4 0.7 all-gather.5.cloned.1.call-update
  179.1 21.0 %reduce-scatter.3.cloned.1.call-done = bf16[768,2048]{1,0:T(8,128)(2,1)} async-done(((bf16[1536,2048]{1,0:T(8,128)(2,1)}), bf16[768,2048]{1,0:T(8,128)(2,1)}) %reduce-scatter.3.cloned.1.call-update) | async-done | bytes 3145744 | tf_op jit(solution)/shard_map/reduce_scatter | solution.py:80
  200.1 6.2 %reshape.61 = bf16[128,6,2048]{2,1,0:T(8,128)(2,1)} reshape(bf16[768,2048]{1,0:T(8,128)(2,1)} %reduce-scatter.3.cloned.1.call-done) | data formatting | bytes 6291456 | tf_op jit(solution)/shard_map/reshape | solution.py:84
  206.3 0.0 copy-start.9
  206.3 14.3 %all-to-all-start.1 = ((bf16[128,6,2048]{2,1,0:T(8,128)(2,1)}), bf16[128,6,2048]{2,1,0:T(8,128)(2,1)}, u32[]{:S(2)}, u32[]{:S(2)}) async-start(bf16[128,6,2048]{2,1,0:T(8,128)(2,1)} %reshape.61), calls=%async_computation.2 | async-start | bytes 8388608 | tf_op jit(solution)/shard_map/all_to_all | solution.py:83
  220.7 0.3 reduce-scatter.5.cloned.1.call-start
  220.9 0.0 all-gather.5.cloned.1.call-done
  220.9 0.0 copy-done.9
  221.0 0.0 copy-start.6
  221.0 3.2 fusion.27
  224.2 0.0 copy-done.6
  224.2 5.4 %convolution_convert_fusion.1 = bf16[512,2048]{1,0:T(8,128)(2,1)} fusion(bf16[256,2048]{1,0:T(8,128)(2,1)} %param.19, bf16[512,2048]{1,0:T(8,128)(2,1)S(1)} %copy-done.6, bf16[2048,256]{1,0:T(8,128)(2,1)} %param.18, f32[512,256]{1,0:T(8,128)} %fusion.27), kind=kOutput, calls=%fused_computation.5 | convolution fusion | flops 1075576832 | bytes 6815744 | tf_op jit(solution)/shard_map/dot_general | solution.py:26
  229.6 0.0 copy-start.5
  229.6 0.0 reduce-scatter.5.cloned.1.call-update
  229.6 0.7 copy-done.5
  230.3 0.1 copy.14
  230.4 85.6 %all-to-all-done.1 = bf16[128,6,2048]{2,1,0:T(8,128)(2,1)} async-done(((bf16[128,6,2048]{2,1,0:T(8,128)(2,1)}), bf16[128,6,2048]{2,1,0:T(8,128)(2,1)}, u32[]{:S(2)}, u32[]{:S(2)}) %all-to-all-start.1) | async-done | bytes 3145760 | tf_op jit(solution)/shard_map/all_to_all | solution.py:83
  316.0 4.9 %reshape.62 = bf16[768,2048]{1,0:T(8,128)(2,1)S(1)} reshape(bf16[128,6,2048]{2,1,0:T(8,128)(2,1)} %all-to-all-done.1) | data formatting | bytes 6291456 | tf_op jit(solution)/shard_map/reshape | solution.py:90
  320.9 3.3 gather_fusion.1
  324.2 5.4 %reshape.63 = f32[256,2,2048]{2,1,0:T(2,128)} reshape(bf16[512,2048]{1,0:T(8,128)(2,1)} %gather_fusion.1) | data formatting | bytes 6291456 | tf_op jit(solution)/shard_map/convert_element_type | solution.py:92
  329.7 0.0 copy-start.1
  329.7 8.9 %multiply_reduce_fusion = f32[256,2048]{1,0:T(8,128)S(1)} fusion(f32[256,2,2048]{2,1,0:T(2,128)} %reshape.63, f32[256,2]{1,0:T(8,128)S(1)} %copy.14), kind=kLoop, calls=%fused_computation.4 | loop fusion | flops 1572864 | bytes 6293504 | tf_op jit(solution)/shard_map/reduce_sum | solution.py:91
  338.5 0.0 reduce-scatter.5.cloned.1.call-done
  338.6 2.5 add_convert_fusion
  341.0 0.0 copy-done.1
  (7 shorter events, 0.0 us)
Async XLA Ops:
  6.5 159.5 %copy-start = (bf16[1,256,2048]{2,1,0:T(8,128)(2,1)S(1)}, bf16[1,256,2048]{2,1,0:T(8,128)(2,1)}, u32[]{:S(2)}) copy-start(bf16[1,256,2048]{2,1,0:T(8,128)(2,1)} %param.16) | copy-start | bytes 3145732
  6.5 6.4 %copy-start.3 = (bf16[256,2048]{1,0:T(8,128)(2,1)S(1)}, bf16[256,2048]{1,0:T(8,128)(2,1)}, u32[]{:S(2)}) copy-start(bf16[256,2048]{1,0:T(8,128)(2,1)} %param.10) | copy-start | bytes 3145732
  6.5 6.5 %copy-start.4 = (f32[2048]{0:T(1024)S(1)}, f32[2048]{0:T(1024)}, u32[]{:S(2)}) copy-start(f32[2048]{0:T(1024)} %param.11) | copy-start | bytes 24580
  6.5 153.7 %all-gather.3.cloned.1.call-start = ((), (), s32[]{:S(2)}) async-start(), calls=%async_computation.4 | async-start | bytes 9437184 | tf_op jit(solution)/shard_map/all_gather | solution.py:76
  13.3 4.4 %copy-start.2 = (bf16[256,2048]{1,0:T(8,128)(2,1)}, bf16[256,2048]{1,0:T(8,128)(2,1)S(1)}, u32[]{:S(2)}) copy-start(bf16[256,2048]{1,0:T(8,128)(2,1)S(1)} %fusion.3) | copy-start | bytes 3145732
  141.7 18.6 %copy-start.7 = (bf16[1,2048,256]{2,1,0:T(8,128)(2,1)S(1)}, bf16[1,2048,256]{2,1,0:T(8,128)(2,1)}, u32[]{:S(2)}) copy-start(bf16[1,2048,256]{2,1,0:T(8,128)(2,1)} %param.14) | copy-start | bytes 3145732
  141.7 24.4 %copy-start.8 = (bf16[1,2048,256]{2,1,0:T(8,128)(2,1)S(1)}, bf16[1,2048,256]{2,1,0:T(8,128)(2,1)}, u32[]{:S(2)}) copy-start(bf16[1,2048,256]{2,1,0:T(8,128)(2,1)} %param.15) | copy-start | bytes 3145732
  141.7 58.4 %reduce-scatter.3.cloned.1.call-start = ((), (), s32[]{:S(2)}) async-start(), calls=%async_computation.5 | async-start | bytes 9437184 | tf_op jit(solution)/shard_map/reduce_scatter | solution.py:80
  178.4 42.6 %all-gather.5.cloned.1.call-start = ((), (), s32[]{:S(2)}) async-start(), calls=%async_computation.6 | async-start | bytes 3145728 | tf_op jit(solution)/shard_map/all_gather | solution.py:30
  206.3 14.7 %copy-start.9 = (bf16[2048,256]{1,0:T(8,128)(2,1)S(1)}, bf16[2048,256]{1,0:T(8,128)(2,1)}, u32[]{:S(2)}) copy-start(bf16[2048,256]{1,0:T(8,128)(2,1)} %param.17) | copy-start | bytes 3145732
  206.3 109.7 %all-to-all-start.1 = ((bf16[128,6,2048]{2,1,0:T(8,128)(2,1)}), bf16[128,6,2048]{2,1,0:T(8,128)(2,1)}, u32[]{:S(2)}, u32[]{:S(2)}) async-start(bf16[128,6,2048]{2,1,0:T(8,128)(2,1)} %reshape.61), calls=%async_computation.2 | async-start | bytes 8388608 | tf_op jit(solution)/shard_map/all_to_all | solution.py:83
  220.7 117.9 %reduce-scatter.5.cloned.1.call-start = ((), (), s32[]{:S(2)}) async-start(), calls=%async_computation.7 | async-start | bytes 3145728 | tf_op jit(solution)/shard_map/reduce_scatter | solution.py:31
  221.0 3.3 copy-start.6
  229.6 0.7 copy-start.5
  329.7 11.4 %copy-start.1 = (bf16[1,256,2048]{2,1,0:T(8,128)(2,1)S(1)}, bf16[1,256,2048]{2,1,0:T(8,128)(2,1)}, u32[]{:S(2)}) copy-start(bf16[1,256,2048]{2,1,0:T(8,128)(2,1)} %param.16) | copy-start | bytes 3145732
Sparse Core Ops, SparseCore 0:
  141.8 18.4 all-gather.2
  178.5 21.5 reduce-scatter.2
  201.9 17.1 all-gather.4
  229.7 16.4 reduce-scatter.4
where the time goes:
time: 349 us; the launch traced here: 348 us
  waiting for transfers between devices  126 us (36%)
  blocking collectives  111 us (32%)
  local copies, waits for them, and re-layouts  41.4 us (12%)
  matrix products  27 us (8%)
  starting transfers between devices  14.9 us (4%)
  other arithmetic  13.9 us (4%)
  between operations  13.3 us (4%)
    all_to_all x1, blocking collectives, body(): lax.all_to_all(outgoing, 'ep', split_axis=0, concat_axis=0, tiled=True)  111 us
    all_to_all x1, waiting for transfers between devices, body(): lax.all_to_all(summed.reshape(ep_size, capacity, model_width), 'ep', spli...  85.6 us
    reduce_scatter x1, waiting for transfers between devices, body(): lax.psum_scatter(sliced_term(hidden, down_one).astype(jnp.bfloat16), 'tp'...  21 us
    all_gather x1, waiting for transfers between devices, body(): lax.all_gather(received.reshape(ep_size * capacity, model_width), 'tp', a...  18.4 us
    dot_general x2, matrix products, sliced_term(): jnp.dot(hidden, down_w, preferred_element_type=jnp.float32)  17.7 us
    all_to_all x1, starting transfers between devices, body(): lax.all_to_all(summed.reshape(ep_size, capacity, model_width), 'ep', spli...  14.3 us
    dot_general x2, matrix products, gated_rows(): gate_value = jnp.dot(row_block, gate_w, preferred_element_type=jnp.float32)  9.02 us
    reduce_sum x1, other arithmetic, body(): jnp.sum(gathered.reshape(tok_rows, top_count, model_width).astype(jnp.flo...  8.86 us
  transfers between devices with their start and end apart: 5, of which 3 were waited for; matrix products, arithmetic and copies ran while one was open for 11% of the time, Pallas kernels for 0%

commit v1 on v0

--- a/solution.py
+++ b/solution.py
@@ -4,6 +4,11 @@
 from jax.sharding import PartitionSpec as P
 
 epsilon = 1e-06
+
+
+def gather_by_exchange(array, axis, dim):
+    copies = jnp.concatenate([array] * lax.axis_size(axis), axis=dim)
+    return lax.all_to_all(copies, axis, dim, dim, tiled=True)
 
 
 def normalize(tokens, norm_gain):
@@ -73,7 +78,7 @@
     outgoing = padded[owners].reshape(ep_size, capacity, model_width)
     received = lax.all_to_all(outgoing, "ep", split_axis=0, concat_axis=0, tiled=True)
     hidden = gated_rows(
-        lax.all_gather(received.reshape(ep_size * capacity, model_width), "tp", axis=0, tiled=True),
+        gather_by_exchange(received.reshape(ep_size * capacity, model_width), "tp", 0),
         gate_one,
         up_one,
     )

time: 349 us -> 338 us (0.968)
  waiting for transfers between devices: 126 us -> 102 us
  blocking collectives: 111 us -> 120 us
  other arithmetic: 13.9 us -> 17.8 us
    all_gather x1 -> x0, waiting for transfers between devices: 18.4 us -> none  [body(): lax.all_gather(received.reshape(ep_size * capacity, model_width), 'tp', a...]
    all_to_all x0 -> x1, blocking collectives: none -> 8.92 us  [gather_by_exchange(): return lax.all_to_all(copies, axis, dim, dim, tiled=True)]
    reduce_scatter x1, waiting for transfers between devices: 21 us -> 16 us  [body(): lax.psum_scatter(sliced_term(hidden, down_one).astype(jnp.bfloat16), 'tp'...]
    concatenate x0 -> x1, other arithmetic: none -> 3.96 us  [gather_by_exchange(): copies = jnp.concatenate([array] * lax.axis_size(axis), axis=dim)]
  transfers between devices with their start and end apart: 5 -> 4, of which waited for: 3 -> 2; matrix products, arithmetic and copies ran while one was open for 11% -> 11% of each run, Pallas kernels for 0% -> 0%
where the time goes in v1:
time: 338 us; the launch traced here: 337 us
  blocking collectives  120 us (36%)
  waiting for transfers between devices  102 us (30%)
  local copies, waits for them, and re-layouts  44.1 us (13%)
  matrix products  24.3 us (7%)
  other arithmetic  17.8 us (5%)
  starting transfers between devices  14.7 us (4%)
  between operations  13.3 us (4%)
    all_to_all x1, blocking collectives, body(): lax.all_to_all(outgoing, 'ep', split_axis=0, concat_axis=0, tiled=True)  111 us
    all_to_all x1, waiting for transfers between devices, body(): lax.all_to_all(summed.reshape(ep_size, capacity, model_width), 'ep', spli...  85.6 us
    dot_general x2, matrix products, sliced_term(): jnp.dot(hidden, down_w, preferred_element_type=jnp.float32)  17.7 us
    reduce_scatter x1, waiting for transfers between devices, body(): lax.psum_scatter(sliced_term(hidden, down_one).astype(jnp.bfloat16), 'tp'...  16 us
    all_to_all x1, starting transfers between devices, body(): lax.all_to_all(summed.reshape(ep_size, capacity, model_width), 'ep', spli...  14.4 us
    all_to_all x1, blocking collectives, gather_by_exchange(): return lax.all_to_all(copies, axis, dim, dim, tiled=True)  8.92 us
    reduce_sum x1, other arithmetic, body(): jnp.sum(gathered.reshape(tok_rows, top_count, model_width).astype(jnp.flo...  8.86 us
  transfers between devices with their start and end apart: 4, of which 2 were waited for; matrix products, arithmetic and copies ran while one was open for 11% of the time, Pallas kernels for 0%

profile of v1, /device:TPU:6, one launch (start us, length us, event | category | flops | bytes accessed | tf_op | source)
XLA Modules:
  0.0 336.8 jit_solution(7381680345387789978)
XLA Ops:
  6.5 0.0 copy-start
  6.5 0.0 copy-start.4
  6.5 0.0 copy-start.5
  6.5 0.0 reduce-scatter.3.cloned.1.call-start
  6.5 1.0 copy.13
  7.5 0.7 broadcast_multiply_fusion
  8.2 1.5 fusion.1
  9.7 0.1 eq.15
  9.9 0.3 fusion.5
  10.2 0.1 copy.12
  10.3 0.1 mul.67
  10.5 2.4 scatter_custom_fusion
  13.0 0.0 copy-done.4
  13.0 0.0 copy-done.5
  13.0 0.3 fusion.3
  13.3 0.0 copy-start.2
  13.3 0.1 concatenate.6
  13.4 4.3 %gather_fusion = bf16[768,2048]{1,0:T(8,128)(2,1)} fusion(bf16[257,2048]{1,0:T(8,128)(2,1)S(1)} %concatenate.6, s32[1024]{0:T(1024)S(1)} %pad_clamp_fusion.1), kind=kCustom, calls=%fused_computation | custom fusion | bytes 6294528 | tf_op jit(solution)/shard_map/gather | solution.py:78
  17.7 0.0 copy-done.2
  17.7 6.2 %reshape.61 = bf16[128,6,2048]{2,1,0:T(8,128)(2,1)} reshape(bf16[768,2048]{1,0:T(8,128)(2,1)} %gather_fusion) | data formatting | bytes 6291456 | tf_op jit(solution)/shard_map/reshape | solution.py:78
  24.0 111.4 %all_to_all.22 = bf16[128,6,2048]{2,1,0:T(8,128)(2,1)} all-to-all(bf16[128,6,2048]{2,1,0:T(8,128)(2,1)} %reshape.61), channel_id=1, replica_groups=mesh['ep'=128,'tp'=2] {'ep'}, dimensions={0} | all-to-all | bytes 6291456 | tf_op jit(solution)/shard_map/all_to_all | solution.py:79
  135.3 6.3 %reshape.62 = bf16[768,2048]{1,0:T(8,128)(2,1)} reshape(bf16[128,6,2048]{2,1,0:T(8,128)(2,1)} %all_to_all.22) | data formatting | bytes 6291456 | tf_op jit(solution)/shard_map/reshape | solution.py:81
  141.7 4.0 %pad_maximum_fusion = bf16[1536,2048]{1,0:T(8,128)(2,1)S(1)} fusion(bf16[768,2048]{1,0:T(8,128)(2,1)} %reshape.62), kind=kLoop, calls=%fused_computation.4 | loop fusion | flops 12582912 | bytes 9437184 | tf_op jit(solution)/shard_map/concatenate | solution.py:10
  145.6 0.0 copy-start.8
  145.6 8.9 %all_to_all.23 = bf16[2,768,2048]{2,1,0:T(8,128)(2,1)S(1)} all-to-all(bf16[2,768,2048]{2,1,0:T(8,128)(2,1)S(1)} %bitcast.21), channel_id=1, replica_groups=mesh['ep'=128,'tp'=2] {'tp'}, dimensions={0} | all-to-all | bytes 12582912 | tf_op jit(solution)/shard_map/all_to_all | solution.py:11
  154.6 0.0 copy-start.3
  154.6 2.6 copy-done.3
  157.2 0.0 copy-done.8
  157.2 0.0 copy-start.9
  157.2 3.1 fusion.9
  160.3 0.0 copy-done
  160.3 0.0 copy-done.9
  160.3 12.3 %convolution_convert_fusion = bf16[1536,2048]{1,0:T(8,128)(2,1)} fusion(bf16[1536,2048]{1,0:T(8,128)(2,1)} %bitcast.23, f32[1536,256]{1,0:T(8,128)} %fusion.9, bf16[1,256,2048]{2,1,0:T(8,128)(2,1)S(1)} %copy-done, bf16[1,2048,256]{2,1,0:T(8,128)(2,1)S(1)} %copy-done.9), kind=kOutput, calls=%fused_computation.3 | convolution fusion | flops 3226730496 | bytes 16252928 | tf_op jit(solution)/shard_map/dot_general | solution.py:31
  172.6 0.0 reduce-scatter.3.cloned.1.call-update
  172.6 0.0 all-gather.2.cloned.1.call-start
  172.6 0.7 all-gather.2.cloned.1.call-update
  173.3 16.0 %reduce-scatter.3.cloned.1.call-done = bf16[768,2048]{1,0:T(8,128)(2,1)} async-done(((bf16[1536,2048]{1,0:T(8,128)(2,1)}), bf16[768,2048]{1,0:T(8,128)(2,1)}) %reduce-scatter.3.cloned.1.call-update) | async-done | bytes 3145744 | tf_op jit(solution)/shard_map/reduce_scatter | solution.py:85
  189.3 6.2 %reshape.63 = bf16[128,6,2048]{2,1,0:T(8,128)(2,1)} reshape(bf16[768,2048]{1,0:T(8,128)(2,1)} %reduce-scatter.3.cloned.1.call-done) | data formatting | bytes 6291456 | tf_op jit(solution)/shard_map/reshape | solution.py:89
  195.6 0.0 copy-start.10
  195.6 14.4 %all-to-all-start.2 = ((bf16[128,6,2048]{2,1,0:T(8,128)(2,1)}), bf16[128,6,2048]{2,1,0:T(8,128)(2,1)}, u32[]{:S(2)}, u32[]{:S(2)}) async-start(bf16[128,6,2048]{2,1,0:T(8,128)(2,1)} %reshape.63), calls=%async_computation.3 | async-start | bytes 8388608 | tf_op jit(solution)/shard_map/all_to_all | solution.py:88
  209.9 0.3 reduce-scatter.5.cloned.1.call-start
  210.2 0.0 all-gather.2.cloned.1.call-done
  210.2 0.0 copy-done.10
  210.3 0.0 copy-start.7
  210.3 3.2 fusion.27
  213.5 0.0 copy-done.7
  213.5 5.4 %convolution_convert_fusion.1 = bf16[512,2048]{1,0:T(8,128)(2,1)} fusion(bf16[256,2048]{1,0:T(8,128)(2,1)} %param.19, bf16[512,2048]{1,0:T(8,128)(2,1)S(1)} %copy-done.7, bf16[2048,256]{1,0:T(8,128)(2,1)} %param.18, f32[512,256]{1,0:T(8,128)} %fusion.27), kind=kOutput, calls=%fused_computation.6 | convolution fusion | flops 1075576832 | bytes 6815744 | tf_op jit(solution)/shard_map/dot_general | solution.py:31
  218.9 0.0 copy-start.6
  218.9 0.0 reduce-scatter.5.cloned.1.call-update
  218.9 0.7 copy-done.6
  219.6 0.1 copy.14
  219.7 85.6 %all-to-all-done.2 = bf16[128,6,2048]{2,1,0:T(8,128)(2,1)} async-done(((bf16[128,6,2048]{2,1,0:T(8,128)(2,1)}), bf16[128,6,2048]{2,1,0:T(8,128)(2,1)}, u32[]{:S(2)}, u32[]{:S(2)}) %all-to-all-start.2) | async-done | bytes 3145760 | tf_op jit(solution)/shard_map/all_to_all | solution.py:88
  305.3 4.9 %reshape.64 = bf16[768,2048]{1,0:T(8,128)(2,1)S(1)} reshape(bf16[128,6,2048]{2,1,0:T(8,128)(2,1)} %all-to-all-done.2) | data formatting | bytes 6291456 | tf_op jit(solution)/shard_map/reshape | solution.py:95
  310.2 3.3 gather_fusion.1
  313.5 5.4 %reshape.65 = f32[256,2,2048]{2,1,0:T(2,128)} reshape(bf16[512,2048]{1,0:T(8,128)(2,1)} %gather_fusion.1) | data formatting | bytes 6291456 | tf_op jit(solution)/shard_map/convert_element_type | solution.py:97
  318.9 0.0 copy-start.1
  318.9 8.9 %multiply_reduce_fusion = f32[256,2048]{1,0:T(8,128)S(1)} fusion(f32[256,2,2048]{2,1,0:T(2,128)} %reshape.65, f32[256,2]{1,0:T(8,128)S(1)} %copy.14), kind=kLoop, calls=%fused_computation.5 | loop fusion | flops 1572864 | bytes 6293504 | tf_op jit(solution)/shard_map/reduce_sum | solution.py:96
  327.8 0.0 reduce-scatter.5.cloned.1.call-done
  327.8 2.5 add_convert_fusion
  330.3 0.0 copy-done.1
  (7 shorter events, 0.0 us)
Async XLA Ops:
  6.5 153.7 %copy-start = (bf16[1,256,2048]{2,1,0:T(8,128)(2,1)S(1)}, bf16[1,256,2048]{2,1,0:T(8,128)(2,1)}, u32[]{:S(2)}) copy-start(bf16[1,256,2048]{2,1,0:T(8,128)(2,1)} %param.16) | copy-start | bytes 3145732
  6.5 6.4 %copy-start.4 = (bf16[256,2048]{1,0:T(8,128)(2,1)S(1)}, bf16[256,2048]{1,0:T(8,128)(2,1)}, u32[]{:S(2)}) copy-start(bf16[256,2048]{1,0:T(8,128)(2,1)} %param.10) | copy-start | bytes 3145732
  6.5 6.5 %copy-start.5 = (f32[2048]{0:T(1024)S(1)}, f32[2048]{0:T(1024)}, u32[]{:S(2)}) copy-start(f32[2048]{0:T(1024)} %param.11) | copy-start | bytes 24580
  6.5 182.8 %reduce-scatter.3.cloned.1.call-start = ((), (), s32[]{:S(2)}) async-start(), calls=%async_computation.5 | async-start | bytes 9437184 | tf_op jit(solution)/shard_map/reduce_scatter | solution.py:85
  13.3 4.4 %copy-start.2 = (bf16[256,2048]{1,0:T(8,128)(2,1)}, bf16[256,2048]{1,0:T(8,128)(2,1)S(1)}, u32[]{:S(2)}) copy-start(bf16[256,2048]{1,0:T(8,128)(2,1)S(1)} %fusion.3) | copy-start | bytes 3145732
  145.6 11.6 %copy-start.8 = (bf16[1,2048,256]{2,1,0:T(8,128)(2,1)S(1)}, bf16[1,2048,256]{2,1,0:T(8,128)(2,1)}, u32[]{:S(2)}) copy-start(bf16[1,2048,256]{2,1,0:T(8,128)(2,1)} %param.14) | copy-start | bytes 3145732
  154.6 2.6 copy-start.3
  157.2 3.1 copy-start.9
  172.6 37.6 %all-gather.2.cloned.1.call-start = ((), (), s32[]{:S(2)}) async-start(), calls=%async_computation.6 | async-start | bytes 3145728 | tf_op jit(solution)/shard_map/all_gather | solution.py:35
  195.6 14.7 %copy-start.10 = (bf16[2048,256]{1,0:T(8,128)(2,1)S(1)}, bf16[2048,256]{1,0:T(8,128)(2,1)}, u32[]{:S(2)}) copy-start(bf16[2048,256]{1,0:T(8,128)(2,1)} %param.17) | copy-start | bytes 3145732
  195.6 109.7 %all-to-all-start.2 = ((bf16[128,6,2048]{2,1,0:T(8,128)(2,1)}), bf16[128,6,2048]{2,1,0:T(8,128)(2,1)}, u32[]{:S(2)}, u32[]{:S(2)}) async-start(bf16[128,6,2048]{2,1,0:T(8,128)(2,1)} %reshape.63), calls=%async_computation.3 | async-start | bytes 8388608 | tf_op jit(solution)/shard_map/all_to_all | solution.py:88
  209.9 117.9 %reduce-scatter.5.cloned.1.call-start = ((), (), s32[]{:S(2)}) async-start(), calls=%async_computation.7 | async-start | bytes 3145728 | tf_op jit(solution)/shard_map/reduce_scatter | solution.py:36
  210.3 3.3 copy-start.7
  218.9 0.7 copy-start.6
  318.9 11.4 %copy-start.1 = (bf16[1,256,2048]{2,1,0:T(8,128)(2,1)S(1)}, bf16[1,256,2048]{2,1,0:T(8,128)(2,1)}, u32[]{:S(2)}) copy-start(bf16[1,256,2048]{2,1,0:T(8,128)(2,1)} %param.16) | copy-start | bytes 3145732
Sparse Core Ops, SparseCore 0:
  172.7 16.5 reduce-scatter.2
  191.1 17.2 all-gather.1
  219.0 16.4 reduce-scatter.4
